TPU v7x, 32 devices: a whole 2x2x4 slice. The times are simulated.
32 devices in a mesh: grp: 2 (over y), ep: 8 (over z, x), tp: 2 (over core).
Axes of the slice: x: 2, y: 2, z: 4, core: 2. Of those that a mesh axis runs over, the one named last changes fastest.
Arguments:
- tokens: bfloat16 [512, 2048], P(('grp', 'ep'), 'tp'), parts along dimension 0, may hold values from -6 to 6
- gain: float32 [2048], replicated, may hold values from 0.1 to 1.9
- routes: int32 [512, 4], P(('grp', 'ep')), parts along dimension 0, may hold values from 0 to 7, all different within a row; in each aligned block of 32 rows (0 to 31, 32 to 63, ...) at most 32 rows name the same one
- weights: float32 [512, 4], P(('grp', 'ep')), parts along dimension 0, may hold values from 0.05 to 1
- w_gate: bfloat16 [8, 2048, 6144], P('ep', None, 'tp'), may hold values from -0.125 to 0.125
- w_up: bfloat16 [8, 2048, 6144], P('ep', None, 'tp'), may hold values from -0.125 to 0.125
- w_down: bfloat16 [8, 6144, 2048], P('ep', 'tp'), may hold values from -0.078125 to 0.078125
Outputs:
- mixed: bfloat16 [512, 2048], P(('grp', 'ep'), 'tp'), parts along dimension 0
There are 2 independent parts, one for each index of `grp`. A program takes and returns all parts, laid end to end along the dimension named above; an argument that names none is the same for every part. Nothing has to cross between parts.
Inputs may be any that keep to these rules, and one draw needn't show every extreme that they name: `routes`: each row names 4 different experts. Among the rows of one device no expert is named by more than 32 rows, a bound that some block reaches.
All inputs are finite; a program needn't handle non-finite values.
Results may differ from a plain program's by a relative error of at most 0.019.
Values may be sent and summed in bfloat16 or wider, within the bound.
No kernel may reach another device: no remote copies, remote signals or barrier semaphores. Data moves between devices by JAX's collectives and lax.ppermute only.
A program may use at most 128 MiB of HBM per device.

v0:
```python
import jax
import jax.numpy as jnp
from jax import lax
from jax.sharding import PartitionSpec as P

epsilon = 1e-05


def expert_rows(chosen, gate_w, up_w, down_w):
    gate_val = jnp.dot(chosen, gate_w, preferred_element_type=jnp.float32)
    up_val = jnp.dot(chosen, up_w, preferred_element_type=jnp.float32)
    hidden = (jax.nn.silu(gate_val) * up_val).astype(jnp.bfloat16)
    partial_value = jnp.dot(hidden, down_w, preferred_element_type=jnp.float32).astype(jnp.bfloat16)
    return (
        lax.psum_scatter(partial_value, "tp", scatter_dimension=1, tiled=True)
        .astype(jnp.float32)
        .astype(jnp.bfloat16)
    )


def on_device(tokens, gain, routes, weights, w_gate, w_up, w_down):
    groups = lax.axis_size("ep")
    shards = lax.axis_size("tp")
    tok_rows, top_count = routes.shape
    capacity = min(tok_rows, 2 * tok_rows * top_count // groups)
    gate_w, up_w, down_w = (w_gate[0], w_up[0], w_down[0])
    values = tokens.astype(jnp.float32)
    own_width = values.shape[1]
    width = own_width * shards
    totals = lax.psum((jnp.sum(values, axis=1), jnp.sum(values * values, axis=1)), "tp")
    average = totals[0] / width
    spread = totals[1] / width - average * average
    local_gain = lax.dynamic_slice_in_dim(gain, lax.axis_index("tp") * own_width, own_width)
    normed = (
        (values - average[:, None]) * lax.rsqrt(spread[:, None] + epsilon) * local_gain
    ).astype(jnp.bfloat16)
    pair_expert = routes.reshape(-1)
    pair_token = jnp.arange(tok_rows * top_count, dtype=jnp.int32) // top_count
    member = (pair_expert[:, None] == jnp.arange(groups, dtype=jnp.int32)[None, :]).astype(
        jnp.int32
    )
    earlier = jnp.cumsum(member, axis=0) - member
    position = pair_expert * capacity + jnp.sum(earlier * member, axis=1)
    row_width = normed.shape[1]
    outbox = (
        jnp.zeros((groups * capacity, row_width), jnp.bfloat16).at[position].set(normed[pair_token])
    )
    outbox = outbox.reshape(groups, capacity, row_width)
    arrived = lax.all_gather(
        lax.all_to_all(outbox, "ep", split_axis=0, concat_axis=0, tiled=True),
        "tp",
        axis=2,
        tiled=True,
    )
    count = arrived.shape[1]
    flat_rows = arrived.reshape(groups * count, arrived.shape[2])
    served = expert_rows(flat_rows, gate_w, up_w, down_w).reshape(groups, count, -1)
    returned = lax.all_to_all(served, "ep", split_axis=0, concat_axis=0, tiled=True)
    picked = (
        returned.reshape(groups * capacity, -1)[position]
        .reshape(tok_rows, top_count, -1)
        .astype(jnp.float32)
    )
    return jnp.sum(picked * weights[:, :, None], axis=1).astype(jnp.bfloat16)


def solution(mesh):
    in_specs = (
        P(("grp", "ep"), "tp"),
        P(),
        P(("grp", "ep"), None),
        P(("grp", "ep"), None),
        P("ep", None, "tp"),
        P("ep", None, "tp"),
        P("ep", "tp", None),
    )
    out_specs = P(("grp", "ep"), "tp")
    return jax.shard_map(
        on_device, mesh=mesh, in_specs=in_specs, out_specs=out_specs, check_vma=False
    )
```

profile of v0, /device:TPU:0, one launch (start us, length us, event | category | flops | bytes accessed | tf_op | source)
XLA Modules:
  0.0 112.8 jit_solution(12843658255355050022)
XLA Ops:
  6.5 0.0 all-gather.2.cloned.1.call-start
  6.5 0.8 copy.12
  7.3 0.7 broadcast_multiply_fusion
  8.0 1.0 convert_reduce_fusion
  9.0 0.1 eq.15
  9.1 0.1 fusion.24
  9.2 0.2 reduce_window_sum.11
  9.3 0.2 select_reduce_fusion
  9.5 0.1 copy.11
  9.6 0.1 mul.57
  9.7 2.6 %all-reduce = (f32[32]{0:T(128)S(1)}, f32[32]{0:T(128)S(1)}) all-reduce(f32[32]{0:T(128)S(1)} %get-tuple-element.6, f32[32]{0:T(128)S(1)} %get-tuple-element.5), channel_id=1, replica_groups=mesh['grp'=2,'ep'=8,'tp'=2] {'tp'}, use_global_device_ids=true, to_apply=%region_5.6 | all-reduce | flops 64 | bytes 512 | tf_op jit(solution)/shard_map/psum | solution.py:30
  12.4 0.7 dynamic_slice.3
  13.1 0.9 fusion.22
  14.0 2.2 %scatter_custom_fusion = bf16[256,1024]{1,0:T(8,128)(2,1)S(1)} fusion(s32[128]{0:T(128)S(1)} %fusion.26, bf16[32,1024]{1,0:T(8,128)(2,1)S(1)} %fusion.22, s32[1024]{0:T(1024)S(1)} %pad_clamp_fusion.1, bf16[]{:T(256)} %constant.34.clone.1), kind=kCustom, calls=%fused_computation.13 | custom fusion | bytes 524290 | tf_op jit(solution)/shard_map/scatter | solution.py:46
  16.2 21.8 %all_to_all.10 = bf16[8,32,1024]{2,1,0:T(8,128)(2,1)} all-to-all(bf16[8,32,1024]{2,1,0:T(8,128)(2,1)S(1)} %bitcast.32), channel_id=1, replica_groups=mesh['grp'=2,'ep'=8,'tp'=2] {'ep'}, dimensions={0} | all-to-all | bytes 1048576 | tf_op jit(solution)/shard_map/all_to_all | solution.py:50
  38.0 0.0 all-gather.2.cloned.1.call-update
  38.1 0.0 reduce-scatter.2.cloned.1.call-start
  38.1 8.2 %all-gather.2.cloned.1.call-done = bf16[8,32,2048]{2,1,0:T(8,128)(2,1)} async-done(((bf16[8,32,1024]{2,1,0:T(8,128)(2,1)}), bf16[8,32,2048]{2,1,0:T(8,128)(2,1)}) %all-gather.2.cloned.1.call-update) | async-done | bytes 1048592 | tf_op jit(solution)/shard_map/all_gather | solution.py:49
  46.3 0.0 copy-start.1
  46.3 10.1 %fusion.4 = f32[256,3072]{1,0:T(8,128)} fusion(bf16[256,2048]{1,0:T(8,128)(2,1)} %bitcast.34, bf16[1,2048,3072]{2,1,0:T(8,128)(2,1)} %param.11), kind=kOutput, calls=%fused_computation.7 | convolution fusion | flops 3221225472 | bytes 16777216 | tf_op jit(solution)/shard_map/dot_general | solution.py:10
  56.4 0.0 copy-done.1
  56.4 0.0 copy-start
  56.4 17.0 %fusion.12 = bf16[256,2048]{1,0:T(8,128)(2,1)} fusion(bf16[1,3072,2048]{2,1,0:T(8,128)(2,1)} %param.13, bf16[256,2048]{1,0:T(8,128)(2,1)S(1)} %bitcast.35, bf16[1,2048,3072]{2,1,0:T(8,128)(2,1)} %param.12, f32[256,3072]{1,0:T(8,128)} %fusion.4), kind=kOutput, calls=%fused_computation.11 | convolution fusion | flops 6447693824 | bytes 30408704 | tf_op jit(solution)/shard_map/dot_general | solution.py:13
  73.4 0.0 reduce-scatter.2.cloned.1.call-update
  73.5 9.7 %reduce-scatter.2.cloned.1.call-done = bf16[256,1024]{1,0:T(8,128)(2,1)} async-done(((bf16[256,2048]{1,0:T(8,128)(2,1)}), bf16[256,1024]{1,0:T(8,128)(2,1)}) %reduce-scatter.2.cloned.1.call-update) | async-done | bytes 524304 | tf_op jit(solution)/shard_map/reduce_scatter | solution.py:15
  83.2 5.8 %all-to-all-start.1 = ((bf16[8,32,1024]{2,1,0:T(8,128)(2,1)}), bf16[8,32,1024]{2,1,0:T(8,128)(2,1)S(1)}, u32[]{:S(2)}, u32[]{:S(2)}) async-start(bf16[8,32,1024]{2,1,0:T(8,128)(2,1)} %bitcast.33), calls=%async_computation.2 | async-start | bytes 1048576 | tf_op jit(solution)/shard_map/all_to_all | solution.py:58
  88.9 0.0 copy-done
  88.9 0.1 copy.13
  89.0 14.8 %all-to-all-done.1 = bf16[8,32,1024]{2,1,0:T(8,128)(2,1)S(1)} async-done(((bf16[8,32,1024]{2,1,0:T(8,128)(2,1)}), bf16[8,32,1024]{2,1,0:T(8,128)(2,1)S(1)}, u32[]{:S(2)}, u32[]{:S(2)}) %all-to-all-start.1) | async-done | bytes 524320 | tf_op jit(solution)/shard_map/all_to_all | solution.py:58
  103.9 0.9 gather_fusion
  104.7 0.2 reshape.98
  104.9 1.0 multiply_reduce_fusion
  (5 shorter events, 0.0 us)
Async XLA Ops:
  6.5 39.8 %all-gather.2.cloned.1.call-start = ((), (), s32[]{:S(2)}) async-start(), calls=%async_computation.3 | async-start | bytes 1572864 | tf_op jit(solution)/shard_map/all_gather | solution.py:49
  38.1 45.1 %reduce-scatter.2.cloned.1.call-start = ((), (), s32[]{:S(2)}) async-start(), calls=%async_computation.4 | async-start | bytes 1572864 | tf_op jit(solution)/shard_map/reduce_scatter | solution.py:15
  46.3 10.1 %copy-start.1 = (bf16[8,32,2048]{2,1,0:T(8,128)(2,1)S(1)}, bf16[8,32,2048]{2,1,0:T(8,128)(2,1)}, u32[]{:S(2)}) copy-start(bf16[8,32,2048]{2,1,0:T(8,128)(2,1)} %all-gather.2.cloned.1.call-done) | copy-start | bytes 3145732
  56.4 32.5 %copy-start = (f32[32,4]{0,1:T(4,128)S(1)}, f32[32,4]{0,1:T(4,128)}, u32[]{:S(2)}) copy-start(f32[32,4]{0,1:T(4,128)} %param.10) | copy-start | bytes 1540
  83.2 20.7 %all-to-all-start.1 = ((bf16[8,32,1024]{2,1,0:T(8,128)(2,1)}), bf16[8,32,1024]{2,1,0:T(8,128)(2,1)S(1)}, u32[]{:S(2)}, u32[]{:S(2)}) async-start(bf16[8,32,1024]{2,1,0:T(8,128)(2,1)} %bitcast.33), calls=%async_computation.2 | async-start | bytes 1048576 | tf_op jit(solution)/shard_map/all_to_all | solution.py:58
Sparse Core Ops, SparseCore 0:
  38.2 8.0 all-gather.1
  73.6 9.5 reduce-scatter.1
where the time goes:
time: 113 us
  waiting for transfers between devices  32.8 us (29%)
  matrix products  27.1 us (24%)
  blocking collectives  24.5 us (22%)
  between operations  13.5 us (12%)
  starting transfers between devices  5.82 us (5%)
  local copies, waits for them, and re-layouts  5.08 us (4%)
  other arithmetic  4.06 us (4%)
    all_to_all x1, blocking collectives, on_device(): lax.all_to_all(outbox, 'ep', split_axis=0, concat_axis=0, tiled=True)  21.8 us
    dot_general x1, matrix products, expert_rows(): jnp.dot(hidden, down_w, preferred_element_type=jnp.float32)  17 us
    all_to_all x1, waiting for transfers between devices, on_device(): lax.all_to_all(served, 'ep', split_axis=0, concat_axis=0, tiled=True)  14.8 us
    dot_general x1, matrix products, expert_rows(): gate_val = jnp.dot(chosen, gate_w, preferred_element_type=jnp.float32)  10.1 us
    reduce_scatter x1, waiting for transfers between devices, expert_rows(): lax.psum_scatter(partial_value, 'tp', scatter_dimension=1, tiled=True)  9.7 us
    all_gather x1, waiting for transfers between devices, on_device(): lax.all_gather(lax.all_to_all(outbox, 'ep', split_axis=0, concat_axis=0,...  8.21 us
    all_to_all x1, starting transfers between devices, on_device(): lax.all_to_all(served, 'ep', split_axis=0, concat_axis=0, tiled=True)  5.78 us
    psum x1, blocking collectives, on_device(): lax.psum((jnp.sum(values, axis=1), jnp.sum(values * values, axis=1)), 'tp')  2.63 us
  transfers between devices with their start and end apart: 3, of which 3 were waited for; matrix products, arithmetic and copies ran while one was open for 0% of the time, Pallas kernels for 0%

commit v1 on v0

--- a/solution.py
+++ b/solution.py
@@ -4,6 +4,36 @@
 from jax.sharding import PartitionSpec as P
 
 epsilon = 1e-05
+
+
+def fill_the_counts(v0, where_dim, page):
+    val2, v_now = (v0.shape[:where_dim], v0.shape[where_dim + 1 :])
+    finding = v0.reshape(*val2, page, -1, *v_now)
+    d_next = jnp.moveaxis(finding, where_dim, 0)
+    return d_next
+
+
+def pieces_all_move(vec, dim_i):
+    vec = jnp.moveaxis(vec, 0, dim_i)
+    a_now = vec.shape
+    met_up = vec.reshape(*a_now[:dim_i], a_now[dim_i] * a_now[dim_i + 1], *a_now[dim_i + 2 :])
+    return met_up
+
+
+def start_the_spots(tile_in, group_axis, a0, block_here):
+    current_arr = lax.psum(1, axis_name=group_axis)
+    frame_out = lax.axis_index(group_axis)
+    t_next, f_now = (current_arr, frame_out)
+    e_now = fill_the_counts(tile_in, a0, t_next)
+    tall = e_now
+    for hop_no in tuple(range(1, t_next)):
+        a_next, all_values = ((f_now + hop_no) % t_next, (f_now - hop_no) % t_next)
+        arr_now = lax.dynamic_index_in_dim(e_now, a_next, 0)
+        carry = tuple(((at, (at + hop_no) % t_next) for at in range(t_next)))
+        base_arr = lax.ppermute(arr_now, axis_name=group_axis, perm=carry)
+        tall = lax.dynamic_update_slice_in_dim(tall, base_arr, all_values, axis=0)
+    v_next = pieces_all_move(tall, block_here)
+    return v_next
 
 
 def expert_rows(chosen, gate_w, up_w, down_w):
@@ -47,10 +77,7 @@
     )
     outbox = outbox.reshape(groups, capacity, row_width)
     arrived = lax.all_gather(
-        lax.all_to_all(outbox, "ep", split_axis=0, concat_axis=0, tiled=True),
-        "tp",
-        axis=2,
-        tiled=True,
+        start_the_spots(outbox, group_axis="ep", a0=0, block_here=0), "tp", axis=2, tiled=True
     )
     count = arrived.shape[1]
     flat_rows = arrived.reshape(groups * count, arrived.shape[2])

time: 113 us -> 111 us (0.982)
  blocking collectives: 24.5 us -> 2.6 us
  starting transfers between devices: 5.82 us -> 19.5 us
  waiting for transfers between devices: 32.8 us -> 38.1 us
    all_to_all x1 -> x0, blocking collectives: 21.8 us -> none  [on_device(): lax.all_to_all(outbox, 'ep', split_axis=0, concat_axis=0, tiled=True)]
    ppermute x0 -> x7, starting transfers between devices: none -> 13.7 us  [start_the_spots(): base_arr = lax.ppermute(arr_now, axis_name=group_axis, perm=carry)]
    ppermute x0 -> x7, waiting for transfers between devices: none -> 3.39 us  [start_the_spots(): base_arr = lax.ppermute(arr_now, axis_name=group_axis, perm=carry)]
    all_gather x1, waiting for transfers between devices: 8.21 us -> 10.1 us  [on_device(): lax.all_gather(start_the_spots(outbox, group_axis='ep', a0=0, block_here=...]
  transfers between devices with their start and end apart: 3 -> 10, of which waited for: 3 -> 7; matrix products, arithmetic and copies ran while one was open for 0% -> 0% of each run, Pallas kernels for 0% -> 0%
where the time goes in v1:
time: 111 us
  waiting for transfers between devices  38.1 us (34%)
  matrix products  27.1 us (24%)
  starting transfers between devices  19.5 us (18%)
  between operations  13.6 us (12%)
  local copies, waits for them, and re-layouts  5.97 us (5%)
  other arithmetic  4.06 us (4%)
  blocking collectives  2.6 us (2%)
    dot_general x1, matrix products, expert_rows(): jnp.dot(hidden, down_w, preferred_element_type=jnp.float32)  17 us
    all_to_all x1, waiting for transfers between devices, on_device(): lax.all_to_all(served, 'ep', split_axis=0, concat_axis=0, tiled=True)  14.9 us
    ppermute x7, starting transfers between devices, start_the_spots(): base_arr = lax.ppermute(arr_now, axis_name=group_axis, perm=carry)  13.7 us
    all_gather x1, waiting for transfers between devices, on_device(): lax.all_gather(start_the_spots(outbox, group_axis='ep', a0=0, block_here=...  10.1 us
    dot_general x1, matrix products, expert_rows(): gate_val = jnp.dot(chosen, gate_w, preferred_element_type=jnp.float32)  10.1 us
    reduce_scatter x1, waiting for transfers between devices, expert_rows(): lax.psum_scatter(partial_value, 'tp', scatter_dimension=1, tiled=True)  9.7 us
    all_to_all x1, starting transfers between devices, on_device(): lax.all_to_all(served, 'ep', split_axis=0, concat_axis=0, tiled=True)  5.77 us
    ppermute x7, waiting for transfers between devices, start_the_spots(): base_arr = lax.ppermute(arr_now, axis_name=group_axis, perm=carry)  3.39 us
  transfers between devices with their start and end apart: 10, of which 7 were waited for; matrix products, arithmetic and copies ran while one was open for 0% of the time, Pallas kernels for 0%

profile of v1, /device:TPU:0, one launch (start us, length us, event | category | flops | bytes accessed | tf_op | source)
XLA Modules:
  0.0 110.9 jit_solution(15109805350046220212)
XLA Ops:
  6.5 0.0 all-gather.2.cloned.1.call-start
  6.5 0.8 copy.12
  7.3 0.7 broadcast_multiply_fusion
  8.0 1.0 convert_reduce_fusion
  8.9 0.1 eq.30
  9.1 0.1 fusion.24
  9.2 0.2 reduce_window_sum.11
  9.3 0.2 select_reduce_fusion
  9.5 0.1 copy.11
  9.6 0.1 mul.57
  9.8 0.7 dynamic_slice.25
  10.5 2.6 %all-reduce = (f32[32]{0:T(128)S(1)}, f32[32]{0:T(128)S(1)}) all-reduce(f32[32]{0:T(128)S(1)} %get-tuple-element.6, f32[32]{0:T(128)S(1)} %get-tuple-element.5), channel_id=1, replica_groups=mesh['grp'=2,'ep'=8,'tp'=2] {'tp'}, use_global_device_ids=true, to_apply=%region_5.6 | all-reduce | flops 64 | bytes 512 | tf_op jit(solution)/shard_map/psum | solution.py:60
  13.1 0.9 fusion.22
  14.0 2.2 %scatter_custom_fusion = bf16[256,1024]{1,0:T(8,128)(2,1)S(1)} fusion(s32[128]{0:T(128)S(1)} %get-tuple-element.19, bf16[32,1024]{1,0:T(8,128)(2,1)S(1)} %fusion.22, s32[1024]{0:T(1024)S(1)} %pad_clamp_fusion.1, bf16[]{:T(256)} %constant.135.clone.1), kind=kCustom, calls=%fused_computation.13 | custom fusion | bytes 524290 | tf_op jit(solution)/shard_map/scatter | solution.py:76
  16.3 2.9 %collective-permute-start = (bf16[1,1,32,1024]{3,2,0,1:T(8,128)(2,1)S(1)}, bf16[1,1,32,1024]{3,2,0,1:T(8,128)(2,1)S(1)}, u32[]{:S(2)}, u32[]{:S(2)}) collective-permute-start(bf16[1,1,32,1024]{3,2,0,1:T(8,128)(2,1)S(1)} %get-tuple-element.15), channel_id=1, source_target_pairs={{0,2},{2,4},{4,6},{6,8},{8,10},{10,12},{12,14},{14,0},{1,3},{3,5},... | collective-permute-start | bytes 196616 | tf_op jit(solution)/shard_map/ppermute | solution.py:33
  19.1 1.6 %collective-permute-start.1 = (bf16[1,1,32,1024]{3,2,0,1:T(8,128)(2,1)S(1)}, bf16[1,1,32,1024]{3,2,0,1:T(8,128)(2,1)S(1)}, u32[]{:S(2)}, u32[]{:S(2)}) collective-permute-start(bf16[1,1,32,1024]{3,2,0,1:T(8,128)(2,1)S(1)} %get-tuple-element.14), channel_id=1, source_target_pairs={{0,4},{2,6},{4,8},{6,10},{8,12},{10,14},{12,0},{14,2},{1,5},{3,7},... | collective-permute-start | bytes 196616 | tf_op jit(solution)/shard_map/ppermute | solution.py:33
  20.7 2.6 %collective-permute-start.2 = (bf16[1,1,32,1024]{3,2,0,1:T(8,128)(2,1)S(1)}, bf16[1,1,32,1024]{3,2,0,1:T(8,128)(2,1)S(1)}, u32[]{:S(2)}, u32[]{:S(2)}) collective-permute-start(bf16[1,1,32,1024]{3,2,0,1:T(8,128)(2,1)S(1)} %get-tuple-element.13), channel_id=1, source_target_pairs={{0,6},{2,8},{4,10},{6,12},{8,14},{10,0},{12,2},{14,4},{1,7},{3,9},... | collective-permute-start | bytes 196616 | tf_op jit(solution)/shard_map/ppermute | solution.py:33
  23.3 1.2 %collective-permute-start.3 = (bf16[1,1,32,1024]{3,2,0,1:T(8,128)(2,1)S(1)}, bf16[1,1,32,1024]{3,2,0,1:T(8,128)(2,1)S(1)}, u32[]{:S(2)}, u32[]{:S(2)}) collective-permute-start(bf16[1,1,32,1024]{3,2,0,1:T(8,128)(2,1)S(1)} %get-tuple-element.12), channel_id=1, source_target_pairs={{0,8},{2,10},{4,12},{6,14},{8,0},{10,2},{12,4},{14,6},{1,9},{3,11}... | collective-permute-start | bytes 196616 | tf_op jit(solution)/shard_map/ppermute | solution.py:33
  24.5 2.6 %collective-permute-start.4 = (bf16[1,1,32,1024]{3,2,0,1:T(8,128)(2,1)S(1)}, bf16[1,1,32,1024]{3,2,0,1:T(8,128)(2,1)S(1)}, u32[]{:S(2)}, u32[]{:S(2)}) collective-permute-start(bf16[1,1,32,1024]{3,2,0,1:T(8,128)(2,1)S(1)} %get-tuple-element.11), channel_id=1, source_target_pairs={{0,10},{2,12},{4,14},{6,0},{8,2},{10,4},{12,6},{14,8},{1,11},{3,13... | collective-permute-start | bytes 196616 | tf_op jit(solution)/shard_map/ppermute | solution.py:33
  27.1 0.0 collective-permute-done
  27.1 1.3 %collective-permute-start.5 = (bf16[1,1,32,1024]{3,2,0,1:T(8,128)(2,1)S(1)}, bf16[1,1,32,1024]{3,2,0,1:T(8,128)(2,1)S(1)}, u32[]{:S(2)}, u32[]{:S(2)}) collective-permute-start(bf16[1,1,32,1024]{3,2,0,1:T(8,128)(2,1)S(1)} %get-tuple-element.10), channel_id=1, source_target_pairs={{0,12},{2,14},{4,0},{6,2},{8,4},{10,6},{12,8},{14,10},{1,13},{3,15... | collective-permute-start | bytes 196616 | tf_op jit(solution)/shard_map/ppermute | solution.py:33
  28.5 0.0 collective-permute-done.1
  28.5 1.5 %collective-permute-start.6 = (bf16[1,1,32,1024]{3,2,0,1:T(8,128)(2,1)S(1)}, bf16[1,1,32,1024]{3,2,0,1:T(8,128)(2,1)S(1)}, u32[]{:S(2)}, u32[]{:S(2)}) collective-permute-start(bf16[1,1,32,1024]{3,2,0,1:T(8,128)(2,1)S(1)} %get-tuple-element.9), channel_id=1, source_target_pairs={{0,14},{2,0},{4,2},{6,4},{8,6},{10,8},{12,10},{14,12},{1,15},{3,1}... | collective-permute-start | bytes 196616 | tf_op jit(solution)/shard_map/ppermute | solution.py:33
  30.0 0.5 collective-permute-done.2
  30.5 0.8 collective-permute-done.3
  31.4 0.9 collective-permute-done.4
  32.3 1.1 %collective-permute-done.5 = bf16[1,1,32,1024]{3,2,0,1:T(8,128)(2,1)S(1)} collective-permute-done((bf16[1,1,32,1024]{3,2,0,1:T(8,128)(2,1)S(1)}, bf16[1,1,32,1024]{3,2,0,1:T(8,128)(2,1)S(1)}, u32[]{:S(2)}, u32[]{:S(2)}) %collective-permute-start.5) | collective-permute-done | bytes 65568 | tf_op jit(solution)/shard_map/ppermute | solution.py:33
  33.4 0.0 collective-permute-done.6
  33.5 0.0 copy-start
  33.5 0.8 copy-done
  34.2 0.0 all-gather.2.cloned.1.call-update
  34.3 0.0 reduce-scatter.2.cloned.1.call-start
  34.3 10.1 %all-gather.2.cloned.1.call-done = bf16[8,32,2048]{2,1,0:T(8,128)(2,1)} async-done(((bf16[8,32,1024]{2,1,0:T(8,128)(2,1)}), bf16[8,32,2048]{2,1,0:T(8,128)(2,1)}) %all-gather.2.cloned.1.call-update) | async-done | bytes 1048592 | tf_op jit(solution)/shard_map/all_gather | solution.py:79
  44.4 0.0 copy-start.2
  44.5 10.1 %fusion.4 = f32[256,3072]{1,0:T(8,128)} fusion(bf16[256,2048]{1,0:T(8,128)(2,1)} %bitcast.50, bf16[1,2048,3072]{2,1,0:T(8,128)(2,1)} %param.11), kind=kOutput, calls=%fused_computation.7 | convolution fusion | flops 3221225472 | bytes 16777216 | tf_op jit(solution)/shard_map/dot_general | solution.py:40
  54.5 0.0 copy-done.2
  54.5 0.0 copy-start.1
  54.5 17.0 %fusion.12 = bf16[256,2048]{1,0:T(8,128)(2,1)} fusion(bf16[1,3072,2048]{2,1,0:T(8,128)(2,1)} %param.13, bf16[256,2048]{1,0:T(8,128)(2,1)S(1)} %bitcast.51, bf16[1,2048,3072]{2,1,0:T(8,128)(2,1)} %param.12, f32[256,3072]{1,0:T(8,128)} %fusion.4), kind=kOutput, calls=%fused_computation.11 | convolution fusion | flops 6447693824 | bytes 30408704 | tf_op jit(solution)/shard_map/dot_general | solution.py:43
  71.6 0.0 reduce-scatter.2.cloned.1.call-update
  71.6 9.7 %reduce-scatter.2.cloned.1.call-done = bf16[256,1024]{1,0:T(8,128)(2,1)} async-done(((bf16[256,2048]{1,0:T(8,128)(2,1)}), bf16[256,1024]{1,0:T(8,128)(2,1)}) %reduce-scatter.2.cloned.1.call-update) | async-done | bytes 524304 | tf_op jit(solution)/shard_map/reduce_scatter | solution.py:45
  81.3 5.8 %all-to-all-start = ((bf16[8,32,1024]{2,1,0:T(8,128)(2,1)}), bf16[8,32,1024]{2,1,0:T(8,128)(2,1)S(1)}, u32[]{:S(2)}, u32[]{:S(2)}) async-start(bf16[8,32,1024]{2,1,0:T(8,128)(2,1)} %bitcast.49), calls=%async_computation.1 | async-start | bytes 1048576 | tf_op jit(solution)/shard_map/all_to_all | solution.py:85
  87.1 0.0 copy-done.1
  87.1 0.1 copy.13
  87.2 14.9 %all-to-all-done = bf16[8,32,1024]{2,1,0:T(8,128)(2,1)S(1)} async-done(((bf16[8,32,1024]{2,1,0:T(8,128)(2,1)}), bf16[8,32,1024]{2,1,0:T(8,128)(2,1)S(1)}, u32[]{:S(2)}, u32[]{:S(2)}) %all-to-all-start) | async-done | bytes 524320 | tf_op jit(solution)/shard_map/all_to_all | solution.py:85
  102.0 0.9 gather_fusion
  102.9 0.2 reshape.134
  103.1 1.0 multiply_reduce_fusion
  (12 shorter events, 0.1 us)
Async XLA Ops:
  6.5 37.9 %all-gather.2.cloned.1.call-start = ((), (), s32[]{:S(2)}) async-start(), calls=%async_computation.2 | async-start | bytes 1572864 | tf_op jit(solution)/shard_map/all_gather | solution.py:79
  16.3 10.9 %collective-permute-start = (bf16[1,1,32,1024]{3,2,0,1:T(8,128)(2,1)S(1)}, bf16[1,1,32,1024]{3,2,0,1:T(8,128)(2,1)S(1)}, u32[]{:S(2)}, u32[]{:S(2)}) collective-permute-start(bf16[1,1,32,1024]{3,2,0,1:T(8,128)(2,1)S(1)} %get-tuple-element.15), channel_id=1, source_target_pairs={{0,2},{2,4},{4,6},{6,8},{8,10},{10,12},{12,14},{14,0},{1,3},{3,5},... | collective-permute-start | bytes 196616 | tf_op jit(solution)/shard_map/ppermute | solution.py:33
  19.1 9.4 %collective-permute-start.1 = (bf16[1,1,32,1024]{3,2,0,1:T(8,128)(2,1)S(1)}, bf16[1,1,32,1024]{3,2,0,1:T(8,128)(2,1)S(1)}, u32[]{:S(2)}, u32[]{:S(2)}) collective-permute-start(bf16[1,1,32,1024]{3,2,0,1:T(8,128)(2,1)S(1)} %get-tuple-element.14), channel_id=1, source_target_pairs={{0,4},{2,6},{4,8},{6,10},{8,12},{10,14},{12,0},{14,2},{1,5},{3,7},... | collective-permute-start | bytes 196616 | tf_op jit(solution)/shard_map/ppermute | solution.py:33
  20.7 9.8 %collective-permute-start.2 = (bf16[1,1,32,1024]{3,2,0,1:T(8,128)(2,1)S(1)}, bf16[1,1,32,1024]{3,2,0,1:T(8,128)(2,1)S(1)}, u32[]{:S(2)}, u32[]{:S(2)}) collective-permute-start(bf16[1,1,32,1024]{3,2,0,1:T(8,128)(2,1)S(1)} %get-tuple-element.13), channel_id=1, source_target_pairs={{0,6},{2,8},{4,10},{6,12},{8,14},{10,0},{12,2},{14,4},{1,7},{3,9},... | collective-permute-start | bytes 196616 | tf_op jit(solution)/shard_map/ppermute | solution.py:33
  23.3 8.1 %collective-permute-start.3 = (bf16[1,1,32,1024]{3,2,0,1:T(8,128)(2,1)S(1)}, bf16[1,1,32,1024]{3,2,0,1:T(8,128)(2,1)S(1)}, u32[]{:S(2)}, u32[]{:S(2)}) collective-permute-start(bf16[1,1,32,1024]{3,2,0,1:T(8,128)(2,1)S(1)} %get-tuple-element.12), channel_id=1, source_target_pairs={{0,8},{2,10},{4,12},{6,14},{8,0},{10,2},{12,4},{14,6},{1,9},{3,11}... | collective-permute-start | bytes 196616 | tf_op jit(solution)/shard_map/ppermute | solution.py:33
  24.5 7.8 %collective-permute-start.4 = (bf16[1,1,32,1024]{3,2,0,1:T(8,128)(2,1)S(1)}, bf16[1,1,32,1024]{3,2,0,1:T(8,128)(2,1)S(1)}, u32[]{:S(2)}, u32[]{:S(2)}) collective-permute-start(bf16[1,1,32,1024]{3,2,0,1:T(8,128)(2,1)S(1)} %get-tuple-element.11), channel_id=1, source_target_pairs={{0,10},{2,12},{4,14},{6,0},{8,2},{10,4},{12,6},{14,8},{1,11},{3,13... | collective-permute-start | bytes 196616 | tf_op jit(solution)/shard_map/ppermute | solution.py:33
  27.1 6.3 %collective-permute-start.5 = (bf16[1,1,32,1024]{3,2,0,1:T(8,128)(2,1)S(1)}, bf16[1,1,32,1024]{3,2,0,1:T(8,128)(2,1)S(1)}, u32[]{:S(2)}, u32[]{:S(2)}) collective-permute-start(bf16[1,1,32,1024]{3,2,0,1:T(8,128)(2,1)S(1)} %get-tuple-element.10), channel_id=1, source_target_pairs={{0,12},{2,14},{4,0},{6,2},{8,4},{10,6},{12,8},{14,10},{1,13},{3,15... | collective-permute-start | bytes 196616 | tf_op jit(solution)/shard_map/ppermute | solution.py:33
  28.5 4.9 %collective-permute-start.6 = (bf16[1,1,32,1024]{3,2,0,1:T(8,128)(2,1)S(1)}, bf16[1,1,32,1024]{3,2,0,1:T(8,128)(2,1)S(1)}, u32[]{:S(2)}, u32[]{:S(2)}) collective-permute-start(bf16[1,1,32,1024]{3,2,0,1:T(8,128)(2,1)S(1)} %get-tuple-element.9), channel_id=1, source_target_pairs={{0,14},{2,0},{4,2},{6,4},{8,6},{10,8},{12,10},{14,12},{1,15},{3,1}... | collective-permute-start | bytes 196616 | tf_op jit(solution)/shard_map/ppermute | solution.py:33
  33.5 0.8 copy-start
  34.3 47.0 %reduce-scatter.2.cloned.1.call-start = ((), (), s32[]{:S(2)}) async-start(), calls=%async_computation.3 | async-start | bytes 1572864 | tf_op jit(solution)/shard_map/reduce_scatter | solution.py:45
  44.4 10.1 %copy-start.2 = (bf16[8,32,2048]{2,1,0:T(8,128)(2,1)S(1)}, bf16[8,32,2048]{2,1,0:T(8,128)(2,1)}, u32[]{:S(2)}) copy-start(bf16[8,32,2048]{2,1,0:T(8,128)(2,1)} %all-gather.2.cloned.1.call-done) | copy-start | bytes 3145732
  54.5 32.5 %copy-start.1 = (f32[32,4]{0,1:T(4,128)S(1)}, f32[32,4]{0,1:T(4,128)}, u32[]{:S(2)}) copy-start(f32[32,4]{0,1:T(4,128)} %param.10) | copy-start | bytes 1540
  81.3 20.7 %all-to-all-start = ((bf16[8,32,1024]{2,1,0:T(8,128)(2,1)}), bf16[8,32,1024]{2,1,0:T(8,128)(2,1)S(1)}, u32[]{:S(2)}, u32[]{:S(2)}) async-start(bf16[8,32,1024]{2,1,0:T(8,128)(2,1)} %bitcast.49), calls=%async_computation.1 | async-start | bytes 1048576 | tf_op jit(solution)/shard_map/all_to_all | solution.py:85
Sparse Core Ops, SparseCore 0:
  34.4 10.0 all-gather.1
  71.7 9.5 reduce-scatter.1
